TPU v7x, 32 devices: a whole 2x2x4 slice. The times are simulated.
32 devices in a mesh: sp: 8 (over z, core), tp: 4 (over y, x).
Axes of the slice: x: 2, y: 2, z: 4, core: 2. Of those that a mesh axis runs over, the one named last changes fastest.
Arguments:
- stream: bfloat16 [3072, 2048], P('sp', 'tp'), may hold values from -6 to 6
- doc_ids: int32 [3072], P('sp'), may hold values from 0 to 1, never falling along the last dimension, each value on 1 to 2304 neighbouring positions
- w_value: bfloat16 [3, 2048, 2048], P(None, None, 'tp'), may hold values from -0.125 to 0.125
- w_gate: bfloat16 [3, 2048, 2048], P(None, None, 'tp'), may hold values from -0.125 to 0.125
- conv_kernel: bfloat16 [3, 31, 2048], P(None, None, 'tp'), may hold values from -4 to 4
- conv_gain: float32 [3, 2048], replicated, may hold values from 0.1 to 1.9
- conv_shift: float32 [3, 2048], replicated, may hold values from -3 to 3
- w_proj: bfloat16 [3, 2048, 2048], P(None, None, 'tp'), may hold values from -0.125 to 0.125
- out_gain: float32 [3, 2048], replicated, may hold values from 0.1 to 1.9
- out_shift: float32 [3, 2048], replicated, may hold values from -3 to 3
Outputs:
- result: bfloat16 [3072, 2048], P('sp', 'tp')
All inputs are finite; a program needn't handle non-finite values.
Results may differ from a plain program's by a relative error of at most 0.013.
Values may be sent and summed in bfloat16 or wider, within the bound.
A program may use at most 64 MiB of HBM per device.

v0:
```python
import functools

import jax
import jax.numpy as jnp
from jax import lax
from jax.experimental import pallas as pl
from jax.experimental.pallas import tpu as pltpu
from jax.sharding import PartitionSpec as P

KERNEL = 31
HALF = 15
PAD = 16
CHUNK = 128
LANES = 128
ROW_BLOCK = 16
CONV_BLOCK = 32
SUM_BLOCK = 32
ALPHA = 2.0**0.25
EPS = 1e-05
MESH = pl.DeviceIdType.MESH


def sigmoid(v):
    return 0.5 * jnp.tanh(0.5 * v) + 0.5


def silu(v):
    return v * sigmoid(v)


def kernel(
    n,
    n_sp,
    stream,
    docs,
    wv_hbm,
    wg_hbm,
    taps_in,
    conv_gain_in,
    conv_shift_in,
    wp_hbm,
    out_gain_in,
    out_shift_in,
    out,
    conv_gain,
    conv_shift,
    out_gain,
    out_shift,
    wv,
    wg,
    wp,
    hbuf,
    cbuf,
    hn,
    act,
    glu,
    docpad,
    taps,
    zf,
    st_send,
    st_recv,
    partial,
    means,
    scales,
    w_sem,
    s_sem,
    r_sem,
    hs_sem,
    hr_sem,
    ds_sem,
    dr_sem,
    ss_sem,
    sr_sem,
):
    rows, local_d = stream.shape
    layers, width, local_c = wv.shape
    groups = local_c // LANES
    chunks = rows // CHUNK
    half = CHUNK // 2
    relayed = n == 4
    me = lax.axis_index("tp")
    sp = lax.axis_index("sp")
    parity = lax.rem(sp, 2)

    for layer in range(layers):
        for i, (src, dst) in enumerate(((wv_hbm, wv), (wg_hbm, wg), (wp_hbm, wp))):
            pltpu.make_async_copy(src.at[layer], dst.at[layer], w_sem.at[i, layer]).start()

    def wait_weight(i, layer):
        src, dst = ((wv_hbm, wv), (wg_hbm, wg), (wp_hbm, wp))[i]
        pltpu.make_async_copy(src.at[layer], dst.at[layer], w_sem.at[i, layer]).wait()

    barrier = pltpu.get_barrier_semaphore()
    for j in range(1, n):
        pl.semaphore_signal(
            barrier, inc=1, device_id={"tp": lax.rem(me + j, n)}, device_id_type=MESH
        )

    @pl.when(sp > 0)
    def _():
        pl.semaphore_signal(barrier, inc=1, device_id={"sp": sp - 1}, device_id_type=MESH)

    @pl.when(sp < n_sp - 1)
    def _():
        pl.semaphore_signal(barrier, inc=1, device_id={"sp": sp + 1}, device_id_type=MESH)

    docpad[pl.ds(PAD, rows), :] = docs[...]
    taps[:, pl.ds(0, KERNEL), :] = taps_in[...].astype(jnp.float32)
    hbuf[0, me] = stream[...]
    for layer in range(layers):
        conv_gain[layer] = conv_gain_in[pl.ds(layer, 1), :]
        conv_shift[layer] = conv_shift_in[pl.ds(layer, 1), :]
        out_gain[layer] = out_gain_in[pl.ds(layer, 1), :]
        out_shift[layer] = out_shift_in[pl.ds(layer, 1), :]
    if n * 8 < LANES:
        st_recv[:, pl.ds(n * 8, LANES - n * 8), :] = jnp.zeros(
            (chunks, LANES - n * 8, LANES), jnp.float32
        )

    @pl.when(sp == 0)
    def _():
        docpad[pl.ds(0, PAD), :] = jnp.full((PAD, LANES), -1, jnp.int32)
        glu[:, :, pl.ds(0, PAD), :] = jnp.zeros((layers, groups, PAD, LANES), jnp.float32)

    @pl.when(sp == n_sp - 1)
    def _():
        docpad[pl.ds(PAD + rows, PAD), :] = jnp.full((PAD, LANES), -1, jnp.int32)
        glu[:, :, pl.ds(PAD + rows, PAD), :] = jnp.zeros(
            (layers, groups, PAD, LANES), jnp.float32
        )

    beside = (sp > 0).astype(jnp.int32) + (sp < n_sp - 1).astype(jnp.int32)
    pl.semaphore_wait(barrier, n - 1 + beside)

    def first_row(p):
        return pl.multiple_of((p + parity * (chunks - 1 - 2 * p)) * CHUNK, CHUNK)

    starts = [first_row(p) for p in range(chunks)]

    if relayed:
        near_x = me + 1 - 2 * lax.rem(me, 2)
        near_y = me + 2 - 4 * (me // 2)

    def own_copies(buf, layer, kind, p, source=None):
        a = 2 * layer + kind
        if relayed:
            plan = [(near_x, 0, 0), (near_y, half, 1), (near_x, half, 4), (near_y, 0, 5)]
            size = half
        else:
            plan = [(lax.rem(me + j, n), 0, j - 1) for j in range(1, n)]
            size = CHUNK
        copies = []
        for peer, offset, i in plan:
            part = pl.ds(pl.multiple_of(starts[p] + offset, half), size)
            block = buf.at[layer, me, part, :]
            copies.append(
                pltpu.make_async_remote_copy(
                    src_ref=block if source is None else source.at[part, :],
                    dst_ref=block,
                    send_sem=s_sem.at[a, p, i],
                    recv_sem=r_sem.at[a, p, i],
                    device_id={"tp": peer},
                    device_id_type=MESH,
                )
            )
        return copies

    def relay_copies(buf, layer, kind, p):
        a = 2 * layer + kind
        out_copies = []
        for i, (origin, target) in enumerate(((near_x, near_y), (near_y, near_x))):
            part = buf.at[
                layer, origin, pl.ds(pl.multiple_of(starts[p] + i * half, half), half), :
            ]
            out_copies.append(
                pltpu.make_async_remote_copy(
                    src_ref=part,
                    dst_ref=part,
                    send_sem=s_sem.at[a, p, 2 + i],
                    recv_sem=r_sem.at[a, p, 2 + i],
                    device_id={"tp": target},
                    device_id_type=MESH,
                )
            )
        return out_copies

    def send(buf, layer, kind, p, source=None):
        for copy in own_copies(buf, layer, kind, p, source):
            copy.start()

    def relay(buf, layer, kind, p):
        if relayed:
            own = own_copies(buf, layer, kind, p)[:2]
            for copy, onward in zip(own, relay_copies(buf, layer, kind, p)):
                copy.wait_recv()
                onward.start()

    def finish(buf, layer, kind, p):
        if relayed:
            for copy in own_copies(buf, layer, kind, p)[2:] + relay_copies(buf, layer, kind, p):
                copy.wait_recv()
        else:
            for copy in own_copies(buf, layer, kind, p):
                copy.wait_recv()

    def drain(buf, layer, kind, p):
        for copy in own_copies(buf, layer, kind, p):
            copy.wait_send()
        if relayed:
            for copy in relay_copies(buf, layer, kind, p):
                copy.wait_send()

    def edge(e):
        side = lax.rem(parity + e, 2)
        partner = sp - 1 + 2 * side
        there = (partner >= 0) & (partner < n_sp)
        src = pl.multiple_of(PAD + side * (rows - PAD), PAD)
        dst = pl.multiple_of((1 - side) * (PAD + rows), PAD)
        return partner, there, src, dst

    def halo_copy(layer, e):
        partner, there, src, dst = edge(e)
        return there, pltpu.make_async_remote_copy(
            src_ref=glu.at[layer, :, pl.ds(src, PAD), :],
            dst_ref=glu.at[layer, :, pl.ds(dst, PAD), :],
            send_sem=hs_sem.at[layer, e],
            recv_sem=hr_sem.at[layer, e],
            device_id={"sp": partner},
            device_id_type=MESH,
        )

    def doc_copy(e):
        partner, there, src, dst = edge(e)
        return there, pltpu.make_async_remote_copy(
            src_ref=docs.at[pl.ds(pl.multiple_of(src - PAD, PAD), PAD), :],
            dst_ref=docpad.at[pl.ds(dst, PAD), :],
            send_sem=ds_sem.at[e],
            recv_sem=dr_sem.at[e],
            device_id={"sp": partner},
            device_id_type=MESH,
        )

    def on(pair, what):
        there, copy = pair

        @pl.when(there)
        def _():
            getattr(copy, what)()

    def normalize(load, store, gain, shift, piece, finish_with):
        lanes = range(piece // LANES)

        def gather_sum(term):
            def body(i, carry):
                at = pl.multiple_of(i * SUM_BLOCK, SUM_BLOCK)
                total = jnp.zeros((SUM_BLOCK, LANES), jnp.float32)
                for s in range(n):
                    part = load(s, at, SUM_BLOCK)
                    for g in lanes:
                        total = total + term(
                            part[:, g * LANES : (g + 1) * LANES].astype(jnp.float32), at
                        )
                partial[pl.ds(at, SUM_BLOCK), :] = total
                return carry

            lax.fori_loop(0, CHUNK // SUM_BLOCK, body, 0, unroll=2)
            return jnp.sum(partial[...], axis=1, keepdims=True) * (1.0 / width)

        def square(value, at):
            off = value - means[pl.ds(at, SUM_BLOCK), :]
            return off * off

        means[...] = jnp.broadcast_to(gather_sum(lambda value, at: value), (CHUNK, LANES))
        scales[...] = jnp.broadcast_to(lax.rsqrt(gather_sum(square) + EPS), (CHUNK, LANES))

        def body(i, carry):
            at = pl.multiple_of(i * ROW_BLOCK, ROW_BLOCK)
            mean = means[pl.ds(at, ROW_BLOCK), :]
            scale = scales[pl.ds(at, ROW_BLOCK), :]
            for s in range(n):
                part = load(s, at, ROW_BLOCK)
                for g in lanes:
                    value = part[:, g * LANES : (g + 1) * LANES].astype(jnp.float32)
                    column = s * piece + g * LANES
                    value = (value - mean) * scale * gain(column) + shift(column)
                    store(s, at, g * LANES, finish_with(value).astype(jnp.bfloat16))
            return carry

        lax.fori_loop(0, CHUNK // ROW_BLOCK, body, 0, unroll=2)

    def make_glu(layer, p):
        r0 = starts[p]
        span = pl.ds(r0, CHUNK)

        @pl.when(layer == 0)
        def _():
            for s in range(n):
                hn[s, span, :] = hbuf[0, s, span, :]

        @pl.when(layer > 0)
        def _():
            before = jnp.maximum(layer - 1, 0)
            normalize(
                lambda s, at, count: hbuf[layer, s, pl.ds(r0 + at, count), :],
                lambda s, at, c, v: hn.__setitem__(
                    (s, pl.ds(r0 + at, ROW_BLOCK), pl.ds(c, LANES)), v
                ),
                lambda c: out_gain[before, :, pl.ds(c, LANES)],
                lambda c: out_shift[before, :, pl.ds(c, LANES)],
                local_d,
                lambda v: v,
            )

        lin = jnp.zeros((CHUNK, local_c), jnp.float32)
        gat = jnp.zeros((CHUNK, local_c), jnp.float32)
        for s in range(n):
            x = hn[s, span, :]
            k = pl.ds(s * local_d, local_d)
            lin = lin + jnp.dot(x, wv[layer, k, :], preferred_element_type=jnp.float32)
            gat = gat + jnp.dot(x, wg[layer, k, :], preferred_element_type=jnp.float32)
        gated = (lin * sigmoid(gat)).astype(jnp.bfloat16).astype(jnp.float32)
        at = pl.multiple_of(r0 + PAD, PAD)
        for g in range(groups):
            glu[layer, g, pl.ds(at, CHUNK), :] = gated[:, g * LANES : (g + 1) * LANES]

    def convolve(layer, p):
        r0 = starts[p]

        def body(i, carry):
            t0 = pl.multiple_of(r0 + i * CONV_BLOCK, CONV_BLOCK)
            centre = docpad[pl.ds(t0 + PAD, CONV_BLOCK), :]
            totals = [jnp.zeros((CONV_BLOCK, LANES), jnp.float32) for _ in range(groups)]
            for k in range(KERNEL):
                at = pl.ds(t0 + k + PAD - HALF, CONV_BLOCK)
                keep = docpad[at, :] == centre
                for g in range(groups):
                    tap = taps[layer, pl.ds(k, 1), pl.ds(g * LANES, LANES)]
                    totals[g] = totals[g] + jnp.where(keep, glu[layer, g, at, :], 0.0) * tap
            for g in range(groups):
                cbuf[layer, me, pl.ds(t0, CONV_BLOCK), pl.ds(g * LANES, LANES)] = totals[
                    g
                ].astype(jnp.bfloat16)
            return carry

        lax.fori_loop(0, CHUNK // CONV_BLOCK, body, 0)

    def project(layer, p):
        r0 = starts[p]
        span = pl.ds(r0, CHUNK)
        normalize(
            lambda s, at, count: cbuf[layer, s, pl.ds(r0 + at, count), :],
            lambda s, at, c, v: act.__setitem__((s, pl.ds(at, ROW_BLOCK), pl.ds(c, LANES)), v),
            lambda c: conv_gain[layer, :, pl.ds(c, LANES)],
            lambda c: conv_shift[layer, :, pl.ds(c, LANES)],
            local_c,
            silu,
        )
        z = ALPHA * hn[me, span, :].astype(jnp.float32)
        for s in range(n):
            z = z + jnp.dot(
                act[s], wp[layer, pl.ds(s * local_c, local_c), :],
                preferred_element_type=jnp.float32,
            )

        @pl.when(layer < layers - 1)
        def _():
            after = jnp.minimum(layer + 1, layers - 1)
            hbuf[after, me, span, :] = z.astype(jnp.bfloat16)
            send(hbuf, after, 0, p)

        @pl.when(layer == layers - 1)
        def _():
            zf[span, :] = z
            total = jnp.sum(z, axis=1, keepdims=True)
            off = z - total * (1.0 / local_d)
            spread = jnp.sum(off * off, axis=1, keepdims=True)
            lane = lax.broadcasted_iota(jnp.int32, (CHUNK, LANES), 1)
            tile = jnp.where(lane == 0, total, jnp.where(lane == 1, spread, 0.0))
            stats = jnp.transpose(tile)[:8, :]
            st_send[p] = stats
            st_recv[p, pl.ds(pl.multiple_of(me * 8, 8), 8), :] = stats
            for copy in stat_copies(p):
                copy.start()

    def stat_copies(p):
        return [
            pltpu.make_async_remote_copy(
                src_ref=st_send.at[p],
                dst_ref=st_recv.at[p, pl.ds(pl.multiple_of(me * 8, 8), 8), :],
                send_sem=ss_sem.at[p, j - 1],
                recv_sem=sr_sem.at[p, j - 1],
                device_id={"tp": lax.rem(me + j, n)},
                device_id_type=MESH,
            )
            for j in range(1, n)
        ]

    for p in range(chunks):
        send(hbuf, 0, 0, p, source=stream)
    for e in range(2):
        on(doc_copy(e), "start")
    for e in range(2):
        on(doc_copy(e), "wait")

    def one_layer(layer, carry):
        relay(hbuf, layer, 0, 0)
        for p in range(chunks):
            if p + 1 < chunks:
                relay(hbuf, layer, 0, p + 1)
            finish(hbuf, layer, 0, p)
            if p == 0:
                wait_weight(0, layer)
                wait_weight(1, layer)
            make_glu(layer, p)
            if p == 0:
                on(halo_copy(layer, 0), "start")
            if p == chunks - 1:
                on(halo_copy(layer, 1), "start")
            if p == 1:
                on(halo_copy(layer, 0), "wait_recv")
            if p >= 1:
                convolve(layer, p - 1)
                send(cbuf, layer, 1, p - 1)
        if chunks == 1:
            on(halo_copy(layer, 0), "wait_recv")
        on(halo_copy(layer, 1), "wait_recv")
        if chunks > 1:
            relay(cbuf, layer, 1, 0)
        convolve(layer, chunks - 1)
        send(cbuf, layer, 1, chunks - 1)
        wait_weight(2, layer)
        if chunks == 1:
            relay(cbuf, layer, 1, 0)
        for p in range(1, chunks):
            relay(cbuf, layer, 1, p)
        for p in range(chunks):
            finish(cbuf, layer, 1, p)
            project(layer, p)
        return carry

    lax.fori_loop(0, layers, one_layer, 0)

    at_d = pl.ds(pl.multiple_of(me * local_d, LANES), local_d)
    gain = out_gain[layers - 1, :, at_d]
    shift = out_shift[layers - 1, :, at_d]
    for p in range(chunks):
        for copy in stat_copies(p):
            copy.wait_recv()
        stats = jnp.transpose(st_recv[p])
        total = stats[:, 0:1]
        for s in range(1, n):
            total = total + stats[:, 8 * s : 8 * s + 1]
        mean = total * (1.0 / width)
        spread = jnp.zeros_like(mean)
        for s in range(n):
            off = stats[:, 8 * s : 8 * s + 1] * (1.0 / local_d) - mean
            spread = spread + stats[:, 8 * s + 1 : 8 * s + 2] + off * off * local_d
        scale = lax.rsqrt(spread * (1.0 / width) + EPS)
        span = pl.ds(starts[p], CHUNK)
        out[span, :] = ((zf[span, :] - mean) * scale * gain + shift).astype(jnp.bfloat16)

    def drain_layer(layer, carry):
        for p in range(chunks):
            drain(hbuf, layer, 0, p)
            drain(cbuf, layer, 1, p)
        for e in range(2):
            on(halo_copy(layer, e), "wait_send")
        return carry

    lax.fori_loop(0, layers, drain_layer, 0)
    for p in range(chunks):
        for copy in stat_copies(p):
            copy.wait_send()


def on_device(
    n,
    n_sp,
    stream,
    doc_ids,
    w_value,
    w_gate,
    conv_kernel,
    conv_gain,
    conv_shift,
    w_proj,
    out_gain,
    out_shift,
):
    rows, local_d = stream.shape
    layers, width, local_c = w_value.shape
    chunks = rows // CHUNK
    docs = jnp.broadcast_to(doc_ids[:, None], (rows, LANES))
    vmem = pl.BlockSpec(memory_space=pltpu.VMEM)
    hbm = pl.BlockSpec(memory_space=pl.ANY)
    ways = 6 if n == 4 else n - 1
    dma = pltpu.SemaphoreType.DMA
    return pl.pallas_call(
        functools.partial(kernel, n, n_sp),
        out_shape=jax.ShapeDtypeStruct((rows, local_d), jnp.bfloat16),
        in_specs=[vmem, vmem, hbm, hbm, vmem, vmem, vmem, hbm, vmem, vmem],
        out_specs=vmem,
        scratch_shapes=[
            pltpu.VMEM((layers, 1, width), jnp.float32),
            pltpu.VMEM((layers, 1, width), jnp.float32),
            pltpu.VMEM((layers, 1, width), jnp.float32),
            pltpu.VMEM((layers, 1, width), jnp.float32),
            pltpu.VMEM((layers, width, local_c), jnp.bfloat16),
            pltpu.VMEM((layers, width, local_c), jnp.bfloat16),
            pltpu.VMEM((layers, local_c * n, local_d), jnp.bfloat16),
            pltpu.VMEM((layers, n, rows, local_d), jnp.bfloat16),
            pltpu.VMEM((layers, n, rows, local_c), jnp.bfloat16),
            pltpu.VMEM((n, rows, local_d), jnp.bfloat16),
            pltpu.VMEM((n, CHUNK, local_c), jnp.bfloat16),
            pltpu.VMEM((layers, local_c // LANES, rows + 2 * PAD, LANES), jnp.float32),
            pltpu.VMEM((rows + 2 * PAD, LANES), jnp.int32),
            pltpu.VMEM((layers, 32, local_c), jnp.float32),
            pltpu.VMEM((rows, local_d), jnp.float32),
            pltpu.VMEM((chunks, 8, LANES), jnp.float32),
            pltpu.VMEM((chunks, LANES, LANES), jnp.float32),
            pltpu.VMEM((CHUNK, LANES), jnp.float32),
            pltpu.VMEM((CHUNK, LANES), jnp.float32),
            pltpu.VMEM((CHUNK, LANES), jnp.float32),
            dma((3, layers)),
            dma((2 * layers, chunks, ways)),
            dma((2 * layers, chunks, ways)),
            dma((layers, 2)),
            dma((layers, 2)),
            dma((2,)),
            dma((2,)),
            dma((chunks, n - 1)),
            dma((chunks, n - 1)),
        ],
        compiler_params=pltpu.CompilerParams(
            collective_id=0, has_side_effects=True, vmem_limit_bytes=60 * 1024 * 1024
        ),
        name="conv_stack",
    )(
        stream,
        docs,
        w_value,
        w_gate,
        conv_kernel,
        conv_gain,
        conv_shift,
        w_proj,
        out_gain,
        out_shift,
    )


def solution(mesh):
    in_specs = (
        P("sp", "tp"),
        P("sp"),
        P(None, None, "tp"),
        P(None, None, "tp"),
        P(None, None, "tp"),
        P(),
        P(),
        P(None, None, "tp"),
        P(),
        P(),
    )
    return jax.shard_map(
        functools.partial(on_device, mesh.shape["tp"], mesh.shape["sp"]),
        mesh=mesh,
        in_specs=in_specs,
        out_specs=P("sp", "tp"),
        check_vma=False,
    )
```

profile of v0, /device:TPU:0, one launch (start us, length us, event | category | flops | bytes accessed | tf_op | source)
XLA Modules:
  0.0 104.2 jit_solution(7982331858003339463)
XLA Ops:
  0.0 1.5 %broadcast_in_dim.2.docs = s32[384,128]{1,0:T(8,128)} broadcast(s32[384]{0:T(512)} %param.11), dimensions={0} | broadcast | bytes 198144 | tf_op jit(solution)/shard_map/broadcast_in_dim | solution.py:493
  1.5 101.0 %conv_stack.1 = bf16[384,512]{1,0:T(8,128)(2,1)} custom-call(bf16[384,512]{1,0:T(8,128)(2,1)} %stream.1, s32[384,128]{1,0:T(8,128)} %broadcast_in_dim.2.docs, bf16[3,2048,512]{2,1,0:T(8,128)(2,1)} %wv_hbm.1, bf16[3,2048,512]{2,1,0:T(8,128)(2,1)} %wg_hbm.1, bf16[3,31,512]{2,1,0:T(8,128)(2,1)} %taps_in.1, f32[3,2048]{1,0:T(4,128)} %conv_gain_in.1, ...), custom_call_target="tpu_custom_call" | custom-call | tf_op jit(solution)/shard_map/conv_stack/pallas_call | solution.py:498
  102.5 1.8 %copy.12 = bf16[384,512]{1,0:T(8,128)(2,1)} copy(bf16[384,512]{1,0:T(8,128)(2,1)} %conv_stack.1) | data formatting | bytes 786432
where the time goes:
time: 106 us; the launch traced here: 104 us
  Pallas kernels  101 us (95%)
  local copies, waits for them, and re-layouts  3.24 us (3%)
    pallas_call x1, Pallas kernels, on_device(): pl.pallas_call(functools.partial(kernel, n, n_sp), out_shape=jax.ShapeDty...  101 us

commit v1 on v0

--- a/solution.py
+++ b/solution.py
@@ -10,7 +10,7 @@
 KERNEL = 31
 HALF = 15
 PAD = 16
-CHUNK = 128
+CHUNK = 96
 LANES = 128
 ROW_BLOCK = 16
 CONV_BLOCK = 32
@@ -20,6 +20,62 @@
 MESH = pl.DeviceIdType.MESH
 
 
+FIRST = (
+    ("send", 0),
+    ("send", 1),
+    ("hr0", 0),
+    ("hr1", 0),
+    ("send", 2),
+    ("hr0", 1),
+    ("hr1", 1),
+    ("send", 3),
+    ("docs", 0),
+    ("hr1", 2),
+)
+REPEAT = (
+    ("glu", 0, 0),
+    ("hr0", 2, 0),
+    ("glu", 1, 0),
+    ("hr1", 3, 0),
+    ("hr0", 3, 0),
+    ("conv", 0, 0),
+    ("glu", 2, 0),
+    ("conv", 1, 0),
+    ("glu", 3, 0),
+    ("cr1", 0, 0),
+    ("cr0", 0, 0),
+    ("conv", 2, 0),
+    ("cr0", 1, 0),
+    ("cr1", 1, 0),
+    ("conv", 3, 0),
+    ("cr1", 2, 0),
+    ("cr0", 2, 0),
+    ("proj", 0, 0),
+    ("cr0", 3, 0),
+    ("cr1", 3, 0),
+    ("proj", 1, 0),
+    ("hr1", 0, 1),
+    ("proj", 2, 0),
+    ("hr0", 0, 1),
+    ("hr1", 1, 1),
+    ("hr0", 1, 1),
+    ("hr1", 2, 1),
+    ("proj", 3, 0),
+)
+
+
+def plan(chunks):
+    if chunks == 4:
+        return FIRST, REPEAT
+    first = [("send", p) for p in range(chunks)] + [("docs", 0)]
+    repeat = [("hr%d" % i, p, 0) for p in range(chunks) for i in range(2)]
+    repeat += [("glu", p, 0) for p in range(chunks)]
+    repeat += [("conv", p, 0) for p in range(chunks)]
+    repeat += [("cr%d" % i, p, 0) for p in range(chunks) for i in range(2)]
+    repeat += [("proj", p, 0) for p in range(chunks)]
+    return first, repeat
+
+
 def sigmoid(v):
     return 0.5 * jnp.tanh(0.5 * v) + 0.5
 
@@ -31,6 +87,8 @@
 def kernel(
     n,
     n_sp,
+    first,
+    repeat,
     stream,
     docs,
     wv_hbm,
@@ -59,7 +117,6 @@
     zf,
     st_send,
     st_recv,
-    partial,
     means,
     scales,
     w_sem,
@@ -112,10 +169,8 @@
         conv_shift[layer] = conv_shift_in[pl.ds(layer, 1), :]
         out_gain[layer] = out_gain_in[pl.ds(layer, 1), :]
         out_shift[layer] = out_shift_in[pl.ds(layer, 1), :]
-    if n * 8 < LANES:
-        st_recv[:, pl.ds(n * 8, LANES - n * 8), :] = jnp.zeros(
-            (chunks, LANES - n * 8, LANES), jnp.float32
-        )
+    st_send[...] = jnp.zeros((chunks, 8, LANES), jnp.float32)
+    st_recv[...] = jnp.zeros((chunks, LANES, LANES), jnp.float32)
 
     @pl.when(sp == 0)
     def _():
@@ -188,12 +243,10 @@
         for copy in own_copies(buf, layer, kind, p, source):
             copy.start()
 
-    def relay(buf, layer, kind, p):
+    def relay(buf, layer, kind, p, i):
         if relayed:
-            own = own_copies(buf, layer, kind, p)[:2]
-            for copy, onward in zip(own, relay_copies(buf, layer, kind, p)):
-                copy.wait_recv()
-                onward.start()
+            own_copies(buf, layer, kind, p)[i].wait_recv()
+            relay_copies(buf, layer, kind, p)[i].start()
 
     def finish(buf, layer, kind, p):
         if relayed:
@@ -250,28 +303,35 @@
     def normalize(load, store, gain, shift, piece, finish_with):
         lanes = range(piece // LANES)
 
-        def gather_sum(term):
-            def body(i, carry):
-                at = pl.multiple_of(i * SUM_BLOCK, SUM_BLOCK)
-                total = jnp.zeros((SUM_BLOCK, LANES), jnp.float32)
-                for s in range(n):
-                    part = load(s, at, SUM_BLOCK)
-                    for g in lanes:
-                        total = total + term(
-                            part[:, g * LANES : (g + 1) * LANES].astype(jnp.float32), at
-                        )
-                partial[pl.ds(at, SUM_BLOCK), :] = total
-                return carry
-
-            lax.fori_loop(0, CHUNK // SUM_BLOCK, body, 0, unroll=2)
-            return jnp.sum(partial[...], axis=1, keepdims=True) * (1.0 / width)
-
-        def square(value, at):
-            off = value - means[pl.ds(at, SUM_BLOCK), :]
-            return off * off
-
-        means[...] = jnp.broadcast_to(gather_sum(lambda value, at: value), (CHUNK, LANES))
-        scales[...] = jnp.broadcast_to(lax.rsqrt(gather_sum(square) + EPS), (CHUNK, LANES))
+        count = width // LANES
+
+        def measure(i, carry):
+            at = pl.multiple_of(i * SUM_BLOCK, SUM_BLOCK)
+            pivot = None
+            for s in range(n):
+                part = load(s, at, SUM_BLOCK)
+                for g in lanes:
+                    value = part[:, g * LANES : (g + 1) * LANES].astype(jnp.float32)
+                    if pivot is None:
+                        pivot = value
+                        first = jnp.zeros_like(value)
+                        second = jnp.zeros_like(value)
+                    else:
+                        off = value - pivot
+                        first = first + off
+                        second = second + off * off
+            middle = first * (1.0 / count)
+            means[pl.ds(at, SUM_BLOCK), :] = pivot + middle
+            scales[pl.ds(at, SUM_BLOCK), :] = jnp.maximum(second - first * middle, 0.0)
+            return carry
+
+        lax.fori_loop(0, CHUNK // SUM_BLOCK, measure, 0, unroll=True)
+        middle = means[...]
+        mean = jnp.sum(middle, axis=1, keepdims=True) * (1.0 / LANES)
+        off = middle - mean
+        spread = jnp.sum(scales[...] + off * off * count, axis=1, keepdims=True)
+        means[...] = jnp.broadcast_to(mean, (CHUNK, LANES))
+        scales[...] = jnp.broadcast_to(lax.rsqrt(spread * (1.0 / width) + EPS), (CHUNK, LANES))
 
         def body(i, carry):
             at = pl.multiple_of(i * ROW_BLOCK, ROW_BLOCK)
@@ -295,7 +355,7 @@
         @pl.when(layer == 0)
         def _():
             for s in range(n):
-                hn[s, span, :] = hbuf[0, s, span, :]
+                hn[span, pl.ds(s * local_d, local_d)] = hbuf[0, s, span, :]
 
         @pl.when(layer > 0)
         def _():
@@ -303,7 +363,7 @@
             normalize(
                 lambda s, at, count: hbuf[layer, s, pl.ds(r0 + at, count), :],
                 lambda s, at, c, v: hn.__setitem__(
-                    (s, pl.ds(r0 + at, ROW_BLOCK), pl.ds(c, LANES)), v
+                    (pl.ds(r0 + at, ROW_BLOCK), pl.ds(s * local_d + c, LANES)), v
                 ),
                 lambda c: out_gain[before, :, pl.ds(c, LANES)],
                 lambda c: out_shift[before, :, pl.ds(c, LANES)],
@@ -311,13 +371,9 @@
                 lambda v: v,
             )
 
-        lin = jnp.zeros((CHUNK, local_c), jnp.float32)
-        gat = jnp.zeros((CHUNK, local_c), jnp.float32)
-        for s in range(n):
-            x = hn[s, span, :]
-            k = pl.ds(s * local_d, local_d)
-            lin = lin + jnp.dot(x, wv[layer, k, :], preferred_element_type=jnp.float32)
-            gat = gat + jnp.dot(x, wg[layer, k, :], preferred_element_type=jnp.float32)
+        x = hn[span, :]
+        lin = jnp.dot(x, wv[layer], preferred_element_type=jnp.float32)
+        gat = jnp.dot(x, wg[layer], preferred_element_type=jnp.float32)
         gated = (lin * sigmoid(gat)).astype(jnp.bfloat16).astype(jnp.float32)
         at = pl.multiple_of(r0 + PAD, PAD)
         for g in range(groups):
@@ -349,18 +405,17 @@
         span = pl.ds(r0, CHUNK)
         normalize(
             lambda s, at, count: cbuf[layer, s, pl.ds(r0 + at, count), :],
-            lambda s, at, c, v: act.__setitem__((s, pl.ds(at, ROW_BLOCK), pl.ds(c, LANES)), v),
+            lambda s, at, c, v: act.__setitem__(
+                (pl.ds(at, ROW_BLOCK), pl.ds(s * local_c + c, LANES)), v
+            ),
             lambda c: conv_gain[layer, :, pl.ds(c, LANES)],
             lambda c: conv_shift[layer, :, pl.ds(c, LANES)],
             local_c,
             silu,
         )
-        z = ALPHA * hn[me, span, :].astype(jnp.float32)
-        for s in range(n):
-            z = z + jnp.dot(
-                act[s], wp[layer, pl.ds(s * local_c, local_c), :],
-                preferred_element_type=jnp.float32,
-            )
+        z = jnp.dot(act[...], wp[layer], preferred_element_type=jnp.float32)
+        own = hn[span, pl.ds(pl.multiple_of(me * local_d, LANES), local_d)]
+        z = z + ALPHA * own.astype(jnp.float32)
 
         @pl.when(layer < layers - 1)
         def _():
@@ -377,8 +432,8 @@
             lane = lax.broadcasted_iota(jnp.int32, (CHUNK, LANES), 1)
             tile = jnp.where(lane == 0, total, jnp.where(lane == 1, spread, 0.0))
             stats = jnp.transpose(tile)[:8, :]
-            st_send[p] = stats
-            st_recv[p, pl.ds(pl.multiple_of(me * 8, 8), 8), :] = stats
+            st_send[p, :, pl.ds(0, CHUNK)] = stats
+            st_recv[p, pl.ds(pl.multiple_of(me * 8, 8), 8), pl.ds(0, CHUNK)] = stats
             for copy in stat_copies(p):
                 copy.start()
 
@@ -395,18 +450,14 @@
             for j in range(1, n)
         ]
 
-    for p in range(chunks):
-        send(hbuf, 0, 0, p, source=stream)
-    for e in range(2):
-        on(doc_copy(e), "start")
-    for e in range(2):
-        on(doc_copy(e), "wait")
-
-    def one_layer(layer, carry):
-        relay(hbuf, layer, 0, 0)
-        for p in range(chunks):
-            if p + 1 < chunks:
-                relay(hbuf, layer, 0, p + 1)
+    def step(what, p, layer):
+        if what == "send":
+            send(hbuf, 0, 0, p, source=stream)
+        elif what in ("hr0", "hr1"):
+            relay(hbuf, layer, 0, p, int(what[2]))
+        elif what in ("cr0", "cr1"):
+            relay(cbuf, layer, 1, p, int(what[2]))
+        elif what == "glu":
             finish(hbuf, layer, 0, p)
             if p == 0:
                 wait_weight(0, layer)
@@ -416,26 +467,37 @@
                 on(halo_copy(layer, 0), "start")
             if p == chunks - 1:
                 on(halo_copy(layer, 1), "start")
-            if p == 1:
+        elif what == "conv":
+            if p == 0:
                 on(halo_copy(layer, 0), "wait_recv")
-            if p >= 1:
-                convolve(layer, p - 1)
-                send(cbuf, layer, 1, p - 1)
-        if chunks == 1:
-            on(halo_copy(layer, 0), "wait_recv")
-        on(halo_copy(layer, 1), "wait_recv")
-        if chunks > 1:
-            relay(cbuf, layer, 1, 0)
-        convolve(layer, chunks - 1)
-        send(cbuf, layer, 1, chunks - 1)
-        wait_weight(2, layer)
-        if chunks == 1:
-            relay(cbuf, layer, 1, 0)
-        for p in range(1, chunks):
-            relay(cbuf, layer, 1, p)
-        for p in range(chunks):
+            if p == chunks - 1:
+                on(halo_copy(layer, 1), "wait_recv")
+            convolve(layer, p)
+            send(cbuf, layer, 1, p)
+        elif what == "proj":
+            if p == 0:
+                wait_weight(2, layer)
             finish(cbuf, layer, 1, p)
             project(layer, p)
+
+    for what, p in first:
+        if what == "docs":
+            for e in range(2):
+                on(doc_copy(e), "start")
+            for e in range(2):
+                on(doc_copy(e), "wait")
+        else:
+            step(what, p, 0)
+
+    def one_layer(layer, carry):
+        for what, p, ahead in repeat:
+            if ahead:
+
+                @pl.when(layer < layers - 1)
+                def _():
+                    step(what, p, jnp.minimum(layer + 1, layers - 1))
+            else:
+                step(what, p, layer)
         return carry
 
     lax.fori_loop(0, layers, one_layer, 0)
@@ -446,7 +508,7 @@
     for p in range(chunks):
         for copy in stat_copies(p):
             copy.wait_recv()
-        stats = jnp.transpose(st_recv[p])
+        stats = jnp.transpose(st_recv[p])[:CHUNK]
         total = stats[:, 0:1]
         for s in range(1, n):
             total = total + stats[:, 8 * s : 8 * s + 1]
@@ -490,13 +552,14 @@
     rows, local_d = stream.shape
     layers, width, local_c = w_value.shape
     chunks = rows // CHUNK
+    first, repeat = plan(chunks)
     docs = jnp.broadcast_to(doc_ids[:, None], (rows, LANES))
     vmem = pl.BlockSpec(memory_space=pltpu.VMEM)
     hbm = pl.BlockSpec(memory_space=pl.ANY)
     ways = 6 if n == 4 else n - 1
     dma = pltpu.SemaphoreType.DMA
     return pl.pallas_call(
-        functools.partial(kernel, n, n_sp),
+        functools.partial(kernel, n, n_sp, first, repeat),
         out_shape=jax.ShapeDtypeStruct((rows, local_d), jnp.bfloat16),
         in_specs=[vmem, vmem, hbm, hbm, vmem, vmem, vmem, hbm, vmem, vmem],
         out_specs=vmem,
@@ -510,15 +573,14 @@
             pltpu.VMEM((layers, local_c * n, local_d), jnp.bfloat16),
             pltpu.VMEM((layers, n, rows, local_d), jnp.bfloat16),
             pltpu.VMEM((layers, n, rows, local_c), jnp.bfloat16),
-            pltpu.VMEM((n, rows, local_d), jnp.bfloat16),
-            pltpu.VMEM((n, CHUNK, local_c), jnp.bfloat16),
+            pltpu.VMEM((rows, n * local_d), jnp.bfloat16),
+            pltpu.VMEM((CHUNK, n * local_c), jnp.bfloat16),
             pltpu.VMEM((layers, local_c // LANES, rows + 2 * PAD, LANES), jnp.float32),
             pltpu.VMEM((rows + 2 * PAD, LANES), jnp.int32),
             pltpu.VMEM((layers, 32, local_c), jnp.float32),
             pltpu.VMEM((rows, local_d), jnp.float32),
             pltpu.VMEM((chunks, 8, LANES), jnp.float32),
             pltpu.VMEM((chunks, LANES, LANES), jnp.float32),
-            pltpu.VMEM((CHUNK, LANES), jnp.float32),
             pltpu.VMEM((CHUNK, LANES), jnp.float32),
             pltpu.VMEM((CHUNK, LANES), jnp.float32),
             dma((3, layers)),

time: 106 us -> 99.8 us (0.942); the launches traced: 104 us -> 99.6 us
  Pallas kernels: 101 us -> 96.3 us
    pallas_call x1, Pallas kernels: 101 us -> 96.3 us  [on_device(): pl.pallas_call(functools.partial(kernel, n, n_sp, first, repeat), out_sha...]
where the time goes in v1:
time: 99.8 us; the launch traced here: 99.6 us
  Pallas kernels  96.3 us (96%)
  local copies, waits for them, and re-layouts  3.24 us (3%)
    pallas_call x1, Pallas kernels, on_device(): pl.pallas_call(functools.partial(kernel, n, n_sp, first, repeat), out_sha...  96.3 us

profile of v1, /device:TPU:0, one launch (start us, length us, event | category | flops | bytes accessed | tf_op | source)
XLA Modules:
  0.0 99.6 jit_solution(9967946631962967088)
XLA Ops:
  0.0 1.5 %broadcast_in_dim.2.docs = s32[384,128]{1,0:T(8,128)} broadcast(s32[384]{0:T(512)} %param.11), dimensions={0} | broadcast | bytes 198144 | tf_op jit(solution)/shard_map/broadcast_in_dim | solution.py:556
  1.5 96.3 %conv_stack.1 = bf16[384,512]{1,0:T(8,128)(2,1)} custom-call(bf16[384,512]{1,0:T(8,128)(2,1)} %stream.1, s32[384,128]{1,0:T(8,128)} %broadcast_in_dim.2.docs, bf16[3,2048,512]{2,1,0:T(8,128)(2,1)} %wv_hbm.1, bf16[3,2048,512]{2,1,0:T(8,128)(2,1)} %wg_hbm.1, bf16[3,31,512]{2,1,0:T(8,128)(2,1)} %taps_in.1, f32[3,2048]{1,0:T(4,128)} %conv_gain_in.1, ...), custom_call_target="tpu_custom_call" | custom-call | tf_op jit(solution)/shard_map/conv_stack/pallas_call | solution.py:561
  97.8 1.8 %copy.12 = bf16[384,512]{1,0:T(8,128)(2,1)} copy(bf16[384,512]{1,0:T(8,128)(2,1)} %conv_stack.1) | data formatting | bytes 786432

commit v2 on v1

--- a/solution.py
+++ b/solution.py
@@ -10,7 +10,6 @@
 KERNEL = 31
 HALF = 15
 PAD = 16
-CHUNK = 96
 LANES = 128
 ROW_BLOCK = 16
 CONV_BLOCK = 32
@@ -20,6 +19,8 @@
 MESH = pl.DeviceIdType.MESH
 
 
+SIZES = (64, 96, 64, 96, 64)
+DIRECT = ((1, 4),)
 FIRST = (
     ("send", 0),
     ("send", 1),
@@ -29,43 +30,59 @@
     ("hr0", 1),
     ("hr1", 1),
     ("send", 3),
+    ("hr0", 2),
+    ("glu", 0),
+    ("hr1", 2),
+    ("send", 4),
     ("docs", 0),
-    ("hr1", 2),
+    ("glu", 1),
+    ("hr1", 3),
 )
 REPEAT = (
-    ("glu", 0, 0),
-    ("hr0", 2, 0),
-    ("glu", 1, 0),
-    ("hr1", 3, 0),
     ("hr0", 3, 0),
     ("conv", 0, 0),
     ("glu", 2, 0),
+    ("hr1", 4, 0),
+    ("hr0", 4, 0),
     ("conv", 1, 0),
     ("glu", 3, 0),
     ("cr1", 0, 0),
     ("cr0", 0, 0),
     ("conv", 2, 0),
+    ("glu", 4, 0),
     ("cr0", 1, 0),
     ("cr1", 1, 0),
     ("conv", 3, 0),
+    ("proj", 0, 0),
     ("cr1", 2, 0),
     ("cr0", 2, 0),
-    ("proj", 0, 0),
+    ("cr1", 3, 0),
     ("cr0", 3, 0),
-    ("cr1", 3, 0),
+    ("conv", 4, 0),
     ("proj", 1, 0),
+    ("hr0", 0, 1),
     ("hr1", 0, 1),
     ("proj", 2, 0),
-    ("hr0", 0, 1),
+    ("cr0", 4, 0),
+    ("cr1", 4, 0),
+    ("hr0", 1, 1),
     ("hr1", 1, 1),
-    ("hr0", 1, 1),
+    ("proj", 3, 0),
+    ("hr0", 2, 1),
+    ("glu", 0, 1),
     ("hr1", 2, 1),
-    ("proj", 3, 0),
+    ("proj", 4, 0),
+    ("glu", 1, 1),
+    ("hr1", 3, 1),
 )
 
 
+def split(rows):
+    return SIZES if sum(SIZES) == rows else (96,) * (rows // 96)
+
+
 def plan(chunks):
-    if chunks == 4:
+    if chunks == len(SIZES):
         return FIRST, REPEAT
     first = [("send", p) for p in range(chunks)] + [("docs", 0)]
     repeat = [("hr%d" % i, p, 0) for p in range(chunks) for i in range(2)]
@@ -80,8 +97,8 @@
     return 0.5 * jnp.tanh(0.5 * v) + 0.5
 
 
-def silu(v):
-    return v * sigmoid(v)
+def silu_of_half(u):
+    return u * jnp.tanh(u) + u
 
 
 def kernel(
@@ -90,16 +107,22 @@
     first,
     repeat,
     stream,
-    docs,
+    docs_hbm,
     wv_hbm,
     wg_hbm,
+    taps_hbm,
+    conv_gain_hbm,
+    conv_shift_hbm,
+    wp_hbm,
+    out_gain_hbm,
+    out_shift_hbm,
+    out,
+    docs,
     taps_in,
     conv_gain_in,
     conv_shift_in,
-    wp_hbm,
     out_gain_in,
     out_shift_in,
-    out,
     conv_gain,
     conv_shift,
     out_gain,
@@ -119,6 +142,7 @@
     st_recv,
     means,
     scales,
+    in_sem,
     w_sem,
     s_sem,
     r_sem,
@@ -132,16 +156,13 @@
     rows, local_d = stream.shape
     layers, width, local_c = wv.shape
     groups = local_c // LANES
-    chunks = rows // CHUNK
-    half = CHUNK // 2
+    sizes = split(rows)
+    chunks = len(sizes)
+    ends = [sum(sizes[: p + 1]) for p in range(chunks)]
     relayed = n == 4
     me = lax.axis_index("tp")
     sp = lax.axis_index("sp")
     parity = lax.rem(sp, 2)
-
-    for layer in range(layers):
-        for i, (src, dst) in enumerate(((wv_hbm, wv), (wg_hbm, wg), (wp_hbm, wp))):
-            pltpu.make_async_copy(src.at[layer], dst.at[layer], w_sem.at[i, layer]).start()
 
     def wait_weight(i, layer):
         src, dst = ((wv_hbm, wv), (wg_hbm, wg), (wp_hbm, wp))[i]
@@ -161,14 +182,28 @@
     def _():
         pl.semaphore_signal(barrier, inc=1, device_id={"sp": sp + 1}, device_id_type=MESH)
 
-    docpad[pl.ds(PAD, rows), :] = docs[...]
-    taps[:, pl.ds(0, KERNEL), :] = taps_in[...].astype(jnp.float32)
-    hbuf[0, me] = stream[...]
+    loads = [
+        pltpu.make_async_copy(src, dst, in_sem.at[i])
+        for i, (src, dst) in enumerate(
+            (
+                (stream, hbuf.at[0, me]),
+                (docs_hbm, docs),
+                (taps_hbm, taps_in),
+                (conv_gain_hbm, conv_gain_in),
+                (conv_shift_hbm, conv_shift_in),
+                (out_gain_hbm, out_gain_in),
+                (out_shift_hbm, out_shift_in),
+            )
+        )
+    ]
+    for load in loads[:2]:
+        load.start()
     for layer in range(layers):
-        conv_gain[layer] = conv_gain_in[pl.ds(layer, 1), :]
-        conv_shift[layer] = conv_shift_in[pl.ds(layer, 1), :]
-        out_gain[layer] = out_gain_in[pl.ds(layer, 1), :]
-        out_shift[layer] = out_shift_in[pl.ds(layer, 1), :]
+        for i, (src, dst) in enumerate(((wv_hbm, wv), (wg_hbm, wg), (wp_hbm, wp))):
+            pltpu.make_async_copy(src.at[layer], dst.at[layer], w_sem.at[i, layer]).start()
+    for load in loads[2:]:
+        load.start()
+
     st_send[...] = jnp.zeros((chunks, 8, LANES), jnp.float32)
     st_recv[...] = jnp.zeros((chunks, LANES, LANES), jnp.float32)
 
@@ -186,9 +221,10 @@
 
     beside = (sp > 0).astype(jnp.int32) + (sp < n_sp - 1).astype(jnp.int32)
     pl.semaphore_wait(barrier, n - 1 + beside)
+    loads[0].wait()
 
     def first_row(p):
-        return pl.multiple_of((p + parity * (chunks - 1 - 2 * p)) * CHUNK, CHUNK)
+        return pl.multiple_of(ends[p] - sizes[p] + parity * (rows + sizes[p] - 2 * ends[p]), 32)
 
     starts = [first_row(p) for p in range(chunks)]
 
@@ -196,21 +232,22 @@
         near_x = me + 1 - 2 * lax.rem(me, 2)
         near_y = me + 2 - 4 * (me // 2)
 
-    def own_copies(buf, layer, kind, p, source=None):
+    def own_copies(buf, layer, kind, p):
         a = 2 * layer + kind
+        half = sizes[p] // 2
         if relayed:
             plan = [(near_x, 0, 0), (near_y, half, 1), (near_x, half, 4), (near_y, 0, 5)]
             size = half
         else:
             plan = [(lax.rem(me + j, n), 0, j - 1) for j in range(1, n)]
-            size = CHUNK
+            size = sizes[p]
         copies = []
         for peer, offset, i in plan:
-            part = pl.ds(pl.multiple_of(starts[p] + offset, half), size)
+            part = pl.ds(pl.multiple_of(starts[p] + offset, 16), size)
             block = buf.at[layer, me, part, :]
             copies.append(
                 pltpu.make_async_remote_copy(
-                    src_ref=block if source is None else source.at[part, :],
+                    src_ref=block,
                     dst_ref=block,
                     send_sem=s_sem.at[a, p, i],
                     recv_sem=r_sem.at[a, p, i],
@@ -222,10 +259,11 @@
 
     def relay_copies(buf, layer, kind, p):
         a = 2 * layer + kind
+        half = sizes[p] // 2
         out_copies = []
         for i, (origin, target) in enumerate(((near_x, near_y), (near_y, near_x))):
             part = buf.at[
-                layer, origin, pl.ds(pl.multiple_of(starts[p] + i * half, half), half), :
+                layer, origin, pl.ds(pl.multiple_of(starts[p] + i * half, 16), half), :
             ]
             out_copies.append(
                 pltpu.make_async_remote_copy(
@@ -239,14 +277,51 @@
             )
         return out_copies
 
-    def send(buf, layer, kind, p, source=None):
-        for copy in own_copies(buf, layer, kind, p, source):
+    def send(buf, layer, kind, p):
+        for copy in own_copies(buf, layer, kind, p):
             copy.start()
+        maybe, when = routed(layer, kind, p)
+        if maybe:
+
+            @pl.when(when)
+            def _():
+                for copy in far_copies(buf, layer, kind, p):
+                    copy.start()
+
+    def routed(layer, kind, p):
+        return relayed and (kind, p) in DIRECT, layer == layers - 1
+
+    def far_copies(buf, layer, kind, p):
+        a = 2 * layer + kind
+        half = sizes[p] // 2
+        copies = []
+        for i in range(2):
+            part = buf.at[
+                layer, me, pl.ds(pl.multiple_of(starts[p] + i * half, 16), half), :
+            ]
+            copies.append(
+                pltpu.make_async_remote_copy(
+                    src_ref=part,
+                    dst_ref=part,
+                    send_sem=s_sem.at[a, p, 2 + i],
+                    recv_sem=r_sem.at[a, p, 2 + i],
+                    device_id={"tp": 3 - me},
+                    device_id_type=MESH,
+                )
+            )
+        return copies
 
     def relay(buf, layer, kind, p, i):
         if relayed:
             own_copies(buf, layer, kind, p)[i].wait_recv()
-            relay_copies(buf, layer, kind, p)[i].start()
+            maybe, when = routed(layer, kind, p)
+            if maybe:
+
+                @pl.when(jnp.logical_not(when))
+                def _():
+                    relay_copies(buf, layer, kind, p)[i].start()
+            else:
+                relay_copies(buf, layer, kind, p)[i].start()
 
     def finish(buf, layer, kind, p):
         if relayed:
@@ -285,7 +360,7 @@
     def doc_copy(e):
         partner, there, src, dst = edge(e)
         return there, pltpu.make_async_remote_copy(
-            src_ref=docs.at[pl.ds(pl.multiple_of(src - PAD, PAD), PAD), :],
+            src_ref=docpad.at[pl.ds(src, PAD), :],
             dst_ref=docpad.at[pl.ds(dst, PAD), :],
             send_sem=ds_sem.at[e],
             recv_sem=dr_sem.at[e],
@@ -300,7 +375,7 @@
         def _():
             getattr(copy, what)()
 
-    def normalize(load, store, gain, shift, piece, finish_with):
+    def normalize(size, load, store, gain, shift, piece, finish_with):
         lanes = range(piece // LANES)
 
         count = width // LANES
@@ -325,13 +400,16 @@
             scales[pl.ds(at, SUM_BLOCK), :] = jnp.maximum(second - first * middle, 0.0)
             return carry
 
-        lax.fori_loop(0, CHUNK // SUM_BLOCK, measure, 0, unroll=True)
-        middle = means[...]
+        lax.fori_loop(0, size // SUM_BLOCK, measure, 0, unroll=True)
+        every = pl.ds(0, size)
+        middle = means[every, :]
         mean = jnp.sum(middle, axis=1, keepdims=True) * (1.0 / LANES)
         off = middle - mean
-        spread = jnp.sum(scales[...] + off * off * count, axis=1, keepdims=True)
-        means[...] = jnp.broadcast_to(mean, (CHUNK, LANES))
-        scales[...] = jnp.broadcast_to(lax.rsqrt(spread * (1.0 / width) + EPS), (CHUNK, LANES))
+        spread = jnp.sum(scales[every, :] + off * off * count, axis=1, keepdims=True)
+        means[every, :] = jnp.broadcast_to(mean, (size, LANES))
+        scales[every, :] = jnp.broadcast_to(
+            lax.rsqrt(spread * (1.0 / width) + EPS), (size, LANES)
+        )
 
         def body(i, carry):
             at = pl.multiple_of(i * ROW_BLOCK, ROW_BLOCK)
@@ -346,11 +424,12 @@
                     store(s, at, g * LANES, finish_with(value).astype(jnp.bfloat16))
             return carry
 
-        lax.fori_loop(0, CHUNK // ROW_BLOCK, body, 0, unroll=2)
+        lax.fori_loop(0, size // ROW_BLOCK, body, 0, unroll=True)
 
     def make_glu(layer, p):
         r0 = starts[p]
-        span = pl.ds(r0, CHUNK)
+        size = sizes[p]
+        span = pl.ds(r0, size)
 
         @pl.when(layer == 0)
         def _():
@@ -361,6 +440,7 @@
         def _():
             before = jnp.maximum(layer - 1, 0)
             normalize(
+                size,
                 lambda s, at, count: hbuf[layer, s, pl.ds(r0 + at, count), :],
                 lambda s, at, c, v: hn.__setitem__(
                     (pl.ds(r0 + at, ROW_BLOCK), pl.ds(s * local_d + c, LANES)), v
@@ -377,7 +457,7 @@
         gated = (lin * sigmoid(gat)).astype(jnp.bfloat16).astype(jnp.float32)
         at = pl.multiple_of(r0 + PAD, PAD)
         for g in range(groups):
-            glu[layer, g, pl.ds(at, CHUNK), :] = gated[:, g * LANES : (g + 1) * LANES]
+            glu[layer, g, pl.ds(at, size), :] = gated[:, g * LANES : (g + 1) * LANES]
 
     def convolve(layer, p):
         r0 = starts[p]
@@ -398,12 +478,14 @@
                 ].astype(jnp.bfloat16)
             return carry
 
-        lax.fori_loop(0, CHUNK // CONV_BLOCK, body, 0)
+        lax.fori_loop(0, sizes[p] // CONV_BLOCK, body, 0)
 
     def project(layer, p):
         r0 = starts[p]
-        span = pl.ds(r0, CHUNK)
+        size = sizes[p]
+        span = pl.ds(r0, size)
         normalize(
+            size,
             lambda s, at, count: cbuf[layer, s, pl.ds(r0 + at, count), :],
             lambda s, at, c, v: act.__setitem__(
                 (pl.ds(at, ROW_BLOCK), pl.ds(s * local_c + c, LANES)), v
@@ -411,9 +493,9 @@
             lambda c: conv_gain[layer, :, pl.ds(c, LANES)],
             lambda c: conv_shift[layer, :, pl.ds(c, LANES)],
             local_c,
-            silu,
+            silu_of_half,
         )
-        z = jnp.dot(act[...], wp[layer], preferred_element_type=jnp.float32)
+        z = jnp.dot(act[pl.ds(0, size), :], wp[layer], preferred_element_type=jnp.float32)
         own = hn[span, pl.ds(pl.multiple_of(me * local_d, LANES), local_d)]
         z = z + ALPHA * own.astype(jnp.float32)
 
@@ -429,11 +511,11 @@
             total = jnp.sum(z, axis=1, keepdims=True)
             off = z - total * (1.0 / local_d)
             spread = jnp.sum(off * off, axis=1, keepdims=True)
-            lane = lax.broadcasted_iota(jnp.int32, (CHUNK, LANES), 1)
+            lane = lax.broadcasted_iota(jnp.int32, (size, LANES), 1)
             tile = jnp.where(lane == 0, total, jnp.where(lane == 1, spread, 0.0))
             stats = jnp.transpose(tile)[:8, :]
-            st_send[p, :, pl.ds(0, CHUNK)] = stats
-            st_recv[p, pl.ds(pl.multiple_of(me * 8, 8), 8), pl.ds(0, CHUNK)] = stats
+            st_send[p, :, pl.ds(0, size)] = stats
+            st_recv[p, pl.ds(pl.multiple_of(me * 8, 8), 8), pl.ds(0, size)] = stats
             for copy in stat_copies(p):
                 copy.start()
 
@@ -450,9 +532,25 @@
             for j in range(1, n)
         ]
 
+    def prepare():
+        loads[1].wait()
+        for i in range(rows // LANES):
+            row = jnp.broadcast_to(docs[pl.ds(i, 1), :], (LANES, LANES))
+            docpad[pl.ds(PAD + i * LANES, LANES), :] = jnp.transpose(row)
+        for e in range(2):
+            on(doc_copy(e), "start")
+        for load in loads[2:]:
+            load.wait()
+        taps[:, pl.ds(0, KERNEL), :] = taps_in[...].astype(jnp.float32)
+        for layer in range(layers):
+            conv_gain[layer] = 0.5 * conv_gain_in[pl.ds(layer, 1), :]
+            conv_shift[layer] = 0.5 * conv_shift_in[pl.ds(layer, 1), :]
+            out_gain[layer] = out_gain_in[pl.ds(layer, 1), :]
+            out_shift[layer] = out_shift_in[pl.ds(layer, 1), :]
+
     def step(what, p, layer):
         if what == "send":
-            send(hbuf, 0, 0, p, source=stream)
+            send(hbuf, 0, 0, p)
         elif what in ("hr0", "hr1"):
             relay(hbuf, layer, 0, p, int(what[2]))
         elif what in ("cr0", "cr1"):
@@ -482,10 +580,7 @@
 
     for what, p in first:
         if what == "docs":
-            for e in range(2):
-                on(doc_copy(e), "start")
-            for e in range(2):
-                on(doc_copy(e), "wait")
+            prepare()
         else:
             step(what, p, 0)
 
@@ -500,6 +595,8 @@
                 step(what, p, layer)
         return carry
 
+    for e in range(2):
+        on(doc_copy(e), "wait_recv")
     lax.fori_loop(0, layers, one_layer, 0)
 
     at_d = pl.ds(pl.multiple_of(me * local_d, LANES), local_d)
@@ -508,7 +605,7 @@
     for p in range(chunks):
         for copy in stat_copies(p):
             copy.wait_recv()
-        stats = jnp.transpose(st_recv[p])[:CHUNK]
+        stats = jnp.transpose(st_recv[p])[: sizes[p]]
         total = stats[:, 0:1]
         for s in range(1, n):
             total = total + stats[:, 8 * s : 8 * s + 1]
@@ -518,7 +615,7 @@
             off = stats[:, 8 * s : 8 * s + 1] * (1.0 / local_d) - mean
             spread = spread + stats[:, 8 * s + 1 : 8 * s + 2] + off * off * local_d
         scale = lax.rsqrt(spread * (1.0 / width) + EPS)
-        span = pl.ds(starts[p], CHUNK)
+        span = pl.ds(starts[p], sizes[p])
         out[span, :] = ((zf[span, :] - mean) * scale * gain + shift).astype(jnp.bfloat16)
 
     def drain_layer(layer, carry):
@@ -530,6 +627,8 @@
         return carry
 
     lax.fori_loop(0, layers, drain_layer, 0)
+    for e in range(2):
+        on(doc_copy(e), "wait_send")
     for p in range(chunks):
         for copy in stat_copies(p):
             copy.wait_send()
@@ -551,9 +650,10 @@
 ):
     rows, local_d = stream.shape
     layers, width, local_c = w_value.shape
-    chunks = rows // CHUNK
+    sizes = split(rows)
+    chunks, tall = len(sizes), max(sizes)
     first, repeat = plan(chunks)
-    docs = jnp.broadcast_to(doc_ids[:, None], (rows, LANES))
+    docs = doc_ids.reshape(rows // LANES, LANES)
     vmem = pl.BlockSpec(memory_space=pltpu.VMEM)
     hbm = pl.BlockSpec(memory_space=pl.ANY)
     ways = 6 if n == 4 else n - 1
@@ -561,9 +661,15 @@
     return pl.pallas_call(
         functools.partial(kernel, n, n_sp, first, repeat),
         out_shape=jax.ShapeDtypeStruct((rows, local_d), jnp.bfloat16),
-        in_specs=[vmem, vmem, hbm, hbm, vmem, vmem, vmem, hbm, vmem, vmem],
+        in_specs=[hbm] * 10,
         out_specs=vmem,
         scratch_shapes=[
+            pltpu.VMEM(docs.shape, jnp.int32),
+            pltpu.VMEM(conv_kernel.shape, jnp.bfloat16),
+            pltpu.VMEM((layers, width), jnp.float32),
+            pltpu.VMEM((layers, width), jnp.float32),
+            pltpu.VMEM((layers, width), jnp.float32),
+            pltpu.VMEM((layers, width), jnp.float32),
             pltpu.VMEM((layers, 1, width), jnp.float32),
             pltpu.VMEM((layers, 1, width), jnp.float32),
             pltpu.VMEM((layers, 1, width), jnp.float32),
@@ -574,15 +680,16 @@
             pltpu.VMEM((layers, n, rows, local_d), jnp.bfloat16),
             pltpu.VMEM((layers, n, rows, local_c), jnp.bfloat16),
             pltpu.VMEM((rows, n * local_d), jnp.bfloat16),
-            pltpu.VMEM((CHUNK, n * local_c), jnp.bfloat16),
+            pltpu.VMEM((tall, n * local_c), jnp.bfloat16),
             pltpu.VMEM((layers, local_c // LANES, rows + 2 * PAD, LANES), jnp.float32),
             pltpu.VMEM((rows + 2 * PAD, LANES), jnp.int32),
             pltpu.VMEM((layers, 32, local_c), jnp.float32),
             pltpu.VMEM((rows, local_d), jnp.float32),
             pltpu.VMEM((chunks, 8, LANES), jnp.float32),
             pltpu.VMEM((chunks, LANES, LANES), jnp.float32),
-            pltpu.VMEM((CHUNK, LANES), jnp.float32),
-            pltpu.VMEM((CHUNK, LANES), jnp.float32),
+            pltpu.VMEM((tall, LANES), jnp.float32),
+            pltpu.VMEM((tall, LANES), jnp.float32),
+            dma((7,)),
             dma((3, layers)),
             dma((2 * layers, chunks, ways)),
             dma((2 * layers, chunks, ways)),

time: 99.8 us -> 95.4 us (0.956)
  Pallas kernels: 96.3 us -> 93.5 us
  local copies, waits for them, and re-layouts: 3.24 us -> 1.77 us
    pallas_call x1, Pallas kernels: 96.3 us -> 93.5 us  [on_device(): pl.pallas_call(functools.partial(kernel, n, n_sp, first, repeat), out_sha...]
    broadcast_in_dim x1 -> x0, local copies, waits for them, and re-layouts: 1.47 us -> none  [on_device(): docs = jnp.broadcast_to(doc_ids[:, None], (rows, LANES))]
where the time goes in v2:
time: 95.4 us; the launch traced here: 95.3 us
  Pallas kernels  93.5 us (98%)
  local copies, waits for them, and re-layouts  1.77 us (2%)
    pallas_call x1, Pallas kernels, on_device(): pl.pallas_call(functools.partial(kernel, n, n_sp, first, repeat), out_sha...  93.5 us

profile of v2, /device:TPU:0, one launch (start us, length us, event | category | flops | bytes accessed | tf_op | source)
XLA Modules:
  0.0 95.3 jit_solution(2088715140731019542)
XLA Ops:
  0.0 93.5 %conv_stack.1 = bf16[384,512]{1,0:T(8,128)(2,1)} custom-call(bf16[384,512]{1,0:T(8,128)(2,1)} %stream.1, s32[3,128]{1,0:T(4,128)} %bitcast.1, bf16[3,2048,512]{2,1,0:T(8,128)(2,1)} %wv_hbm.1, bf16[3,2048,512]{2,1,0:T(8,128)(2,1)} %wg_hbm.1, bf16[3,31,512]{2,1,0:T(8,128)(2,1)} %taps_hbm.1, f32[3,2048]{1,0:T(4,128)} %conv_gain_hbm.1, ...), custom_call_target="tpu_custom_call" | custom-call | tf_op jit(solution)/shard_map/conv_stack/pallas_call | solution.py:661
  93.5 1.8 %copy.12 = bf16[384,512]{1,0:T(8,128)(2,1)} copy(bf16[384,512]{1,0:T(8,128)(2,1)} %conv_stack.1) | data formatting | bytes 786432

commit v3 on v2

--- a/solution.py
+++ b/solution.py
@@ -20,60 +20,58 @@
 
 
 SIZES = (64, 96, 64, 96, 64)
-DIRECT = ((1, 4),)
+DIRECT = ()
 FIRST = (
     ("send", 0),
     ("send", 1),
+    ("send", 2),
+    ("hr1", 0),
     ("hr0", 0),
-    ("hr1", 0),
-    ("send", 2),
+    ("hr1", 1),
     ("hr0", 1),
-    ("hr1", 1),
+    ("hr1", 2),
     ("send", 3),
     ("hr0", 2),
     ("glu", 0),
-    ("hr1", 2),
     ("send", 4),
     ("docs", 0),
-    ("glu", 1),
-    ("hr1", 3),
 )
 REPEAT = (
+    ("glu", 1, 0),
     ("hr0", 3, 0),
+    ("hr1", 3, 0),
     ("conv", 0, 0),
     ("glu", 2, 0),
     ("hr1", 4, 0),
     ("hr0", 4, 0),
     ("conv", 1, 0),
     ("glu", 3, 0),
-    ("cr1", 0, 0),
-    ("cr0", 0, 0),
     ("conv", 2, 0),
     ("glu", 4, 0),
+    ("cr1", 1, 0),
+    ("cr1", 0, 0),
     ("cr0", 1, 0),
-    ("cr1", 1, 0),
+    ("cr0", 0, 0),
     ("conv", 3, 0),
+    ("conv", 4, 0),
+    ("proj", 1, 0),
     ("proj", 0, 0),
     ("cr1", 2, 0),
     ("cr0", 2, 0),
     ("cr1", 3, 0),
+    ("hr1", 1, 1),
     ("cr0", 3, 0),
-    ("conv", 4, 0),
-    ("proj", 1, 0),
+    ("hr1", 0, 1),
     ("hr0", 0, 1),
-    ("hr1", 0, 1),
-    ("proj", 2, 0),
+    ("hr0", 1, 1),
     ("cr0", 4, 0),
     ("cr1", 4, 0),
-    ("hr0", 1, 1),
-    ("hr1", 1, 1),
+    ("proj", 2, 0),
     ("proj", 3, 0),
-    ("hr0", 2, 1),
     ("glu", 0, 1),
     ("hr1", 2, 1),
+    ("hr0", 2, 1),
     ("proj", 4, 0),
-    ("glu", 1, 1),
-    ("hr1", 3, 1),
 )
 
 
@@ -532,6 +530,8 @@
             for j in range(1, n)
         ]
 
+    lead = [p for what, p, _ in repeat if what == "proj"][0]
+
     def prepare():
         loads[1].wait()
         for i in range(rows // LANES):
@@ -573,7 +573,7 @@
             convolve(layer, p)
             send(cbuf, layer, 1, p)
         elif what == "proj":
-            if p == 0:
+            if p == lead:
                 wait_weight(2, layer)
             finish(cbuf, layer, 1, p)
             project(layer, p)
@@ -660,7 +660,7 @@
     dma = pltpu.SemaphoreType.DMA
     return pl.pallas_call(
         functools.partial(kernel, n, n_sp, first, repeat),
-        out_shape=jax.ShapeDtypeStruct((rows, local_d), jnp.bfloat16),
+        out_shape=pltpu.VMEM((rows, local_d), jnp.bfloat16),
         in_specs=[hbm] * 10,
         out_specs=vmem,
         scratch_shapes=[

time: 95.4 us -> 93.2 us (0.977)
  Pallas kernels: 93.5 us -> 92.3 us
  local copies, waits for them, and re-layouts: 1.77 us -> 0.75 us
    pallas_call x1, Pallas kernels: 93.5 us -> 92.3 us  [on_device(): pl.pallas_call(functools.partial(kernel, n, n_sp, first, repeat), out_sha...]
    unnamed x1, local copies, waits for them, and re-layouts: 1.77 us -> 0.75 us
where the time goes in v3:
time: 93.2 us; the launch traced here: 93.1 us
  Pallas kernels  92.3 us (99%)
    pallas_call x1, Pallas kernels, on_device(): pl.pallas_call(functools.partial(kernel, n, n_sp, first, repeat), out_sha...  92.3 us

profile of v3, /device:TPU:0, one launch (start us, length us, event | category | flops | bytes accessed | tf_op | source)
XLA Modules:
  0.0 93.1 jit_solution(2409043008669683058)
XLA Ops:
  0.0 92.3 %conv_stack.1 = bf16[384,512]{1,0:T(8,128)(2,1)S(1)} custom-call(bf16[384,512]{1,0:T(8,128)(2,1)} %stream.1, s32[3,128]{1,0:T(4,128)} %bitcast.1, bf16[3,2048,512]{2,1,0:T(8,128)(2,1)} %wv_hbm.1, bf16[3,2048,512]{2,1,0:T(8,128)(2,1)} %wg_hbm.1, bf16[3,31,512]{2,1,0:T(8,128)(2,1)} %taps_hbm.1, f32[3,2048]{1,0:T(4,128)} %conv_gain_hbm.1, ...), custom_call_target="tpu_custom_call" | custom-call | tf_op jit(solution)/shard_map/conv_stack/pallas_call | solution.py:661
  92.3 0.7 copy.12

commit v4 on v3

--- a/solution.py
+++ b/solution.py
@@ -476,7 +476,7 @@
                 ].astype(jnp.bfloat16)
             return carry
 
-        lax.fori_loop(0, sizes[p] // CONV_BLOCK, body, 0)
+        lax.fori_loop(0, sizes[p] // CONV_BLOCK, body, 0, unroll=True)
 
     def project(layer, p):
         r0 = starts[p]

time: 93.2 us -> 93.1 us (level)
  no operation moved by 1% of the time
where the time goes in v4:
time: 93.1 us; the launch traced here: 92.9 us
  Pallas kernels  92.2 us (99%)
    pallas_call x1, Pallas kernels, on_device(): pl.pallas_call(functools.partial(kernel, n, n_sp, first, repeat), out_sha...  92.2 us

profile of v4, /device:TPU:0, one launch (start us, length us, event | category | flops | bytes accessed | tf_op | source)
XLA Modules:
  0.0 92.9 jit_solution(6609680172355280115)
XLA Ops:
  0.0 92.2 %conv_stack.1 = bf16[384,512]{1,0:T(8,128)(2,1)S(1)} custom-call(bf16[384,512]{1,0:T(8,128)(2,1)} %stream.1, s32[3,128]{1,0:T(4,128)} %bitcast.1, bf16[3,2048,512]{2,1,0:T(8,128)(2,1)} %wv_hbm.1, bf16[3,2048,512]{2,1,0:T(8,128)(2,1)} %wg_hbm.1, bf16[3,31,512]{2,1,0:T(8,128)(2,1)} %taps_hbm.1, f32[3,2048]{1,0:T(4,128)} %conv_gain_hbm.1, ...), custom_call_target="tpu_custom_call" | custom-call | tf_op jit(solution)/shard_map/conv_stack/pallas_call | solution.py:661
  92.2 0.7 copy.12
